TPU v7x, 32 devices: a whole 2x2x4 slice. The times are simulated.
32 devices in a mesh: dp: 4 (over y, x), kv: 4 (over z), tp: 2 (over core).
Axes of the slice: x: 2, y: 2, z: 4, core: 2. Of those that a mesh axis runs over, the one named last changes fastest.
Arguments:
- hidden: bfloat16 [96, 2, 2048], P('dp', 'tp', 'kv'), may hold values from -6 to 6
- lengths: int32 [32], P('dp'), may hold values from 1 to 3, 42 in all
- state: float32 [32, 16, 128, 128], P(('dp', 'kv', 'tp')), may hold values from -6 to 6
- attn_gain: float32 [4096], replicated, may hold values from 0.1 to 1.9
- w_query: bfloat16 [4096, 2048], P(None, ('kv', 'tp')), may hold values from -0.09375 to 0.09375
- w_key: bfloat16 [4096, 2048], P(None, ('kv', 'tp')), may hold values from -0.09375 to 0.09375
- w_value: bfloat16 [4096, 2048], P(None, ('kv', 'tp')), may hold values from -0.09375 to 0.09375
- w_outgate: bfloat16 [4096, 2048], P(None, ('kv', 'tp')), may hold values from -0.09375 to 0.09375
- w_beta: bfloat16 [4096, 16], replicated, may hold values from -0.09375 to 0.09375
- w_decay: bfloat16 [4096, 16], replicated, may hold values from -0.09375 to 0.09375
- head_decay_rate: float32 [16], replicated, may hold values from 0.02 to 2
- decay_bias: float32 [16], replicated, may hold values from -3 to 1
- head_gain: float32 [128], replicated, may hold values from 0.1 to 1.9
- w_proj: bfloat16 [2048, 2, 2048], P(None, 'tp', 'kv'), may hold values from -0.125 to 0.125
- ffn_gain: float32 [4096], replicated, may hold values from 0.1 to 1.9
- w_gate: bfloat16 [4096, 11264], P('tp', 'kv'), may hold values from -0.09375 to 0.09375
- w_up: bfloat16 [4096, 11264], P('tp', 'kv'), may hold values from -0.09375 to 0.09375
- w_down: bfloat16 [11264, 4096], P('kv', 'tp'), may hold values from -0.078125 to 0.078125
Outputs:
- mixed: bfloat16 [96, 2, 2048], P('dp', 'tp', 'kv')
- new_state: float32 [32, 16, 128, 128], P(('dp', 'kv', 'tp'))
Inputs may be any that keep to these rules, and one draw needn't show every extreme that they name: lengths sum to 42; some sequence has 3.
All inputs are finite; a program needn't handle non-finite values. No bound on the sum of `lengths` on one device may be relied on, other than what follows from the above.
Results may differ from a plain program's by a relative error of at most 0.015.
Values may be sent and summed in bfloat16 or wider, within the bound.
A program may use at most 128 MiB of HBM per device.

v0:
```python
import jax
import jax.numpy as jnp
from jax import lax
from jax.sharding import PartitionSpec as P

D = 4096
HEADS = 16
HEAD = 128
SLOTS = 3


EPS = 1e-06


def recur(loop_carry, query_vector, key, value, beta, logdecay):
    query_scale = query_vector.shape[-1] ** (-0.5)
    output_rows = []
    for state_slot in range(query_vector.shape[0]):
        loop_carry = loop_carry * jnp.exp(logdecay[state_slot])[:, None, None]
        recalled_value = jnp.einsum(
            "jtu,jt->ju", loop_carry, key[state_slot], precision=lax.Precision.HIGHEST
        )
        change = beta[state_slot][:, None] * (value[state_slot] - recalled_value)
        loop_carry = loop_carry + key[state_slot][:, :, None] * change[:, None, :]
        output_rows.append(
            jnp.einsum(
                "jtu,jt->ju", loop_carry, query_vector[state_slot], precision=lax.Precision.HIGHEST
            )
            * query_scale
        )
    return (loop_carry, jnp.stack(output_rows))


def unit_rows(values):
    return values * lax.rsqrt(jnp.sum(values * values, axis=-1, keepdims=True) + EPS)


def local(
    hidden,
    lengths,
    state,
    attn_gain,
    w_query,
    w_key,
    w_value,
    w_outgate,
    w_beta,
    w_decay,
    head_decay_rate,
    decay_bias,
    head_gain,
    w_proj,
    ffn_gain,
    w_gate,
    w_up,
    w_down,
):
    rank = lax.axis_index(("kv", "tp"))
    core = lax.axis_index("tp")
    own = state.shape[0]
    own_rows = own * SLOTS
    row_total = hidden.shape[0]
    piece_cols = hidden.shape[2]
    half_cols = piece_cols * lax.axis_size("kv")
    live = (jnp.arange(SLOTS)[None, :] < lengths[:, None]).astype(jnp.float32).reshape(-1)
    own_lengths = lax.dynamic_slice_in_dim(lengths, rank * own, own)
    own_live = (jnp.arange(SLOTS)[None, :] < own_lengths[:, None]).astype(jnp.float32).reshape(-1)
    half_rows = lax.all_gather(hidden, "kv", axis=2, tiled=True)
    whole = lax.all_gather(half_rows, "tp", axis=1, tiled=True).reshape(row_total, -1)
    xf = whole.astype(jnp.float32)
    normed = (xf * lax.rsqrt(jnp.mean(xf * xf, axis=1, keepdims=True) + EPS) * attn_gain).astype(
        jnp.bfloat16
    )
    projected = jnp.stack(
        [
            jnp.dot(normed, weight, preferred_element_type=jnp.float32)
            for weight in (w_query, w_key, w_value, w_outgate)
        ],
        axis=1,
    ).astype(jnp.bfloat16)
    mine = lax.all_to_all(projected, ("kv", "tp"), split_axis=0, concat_axis=2, tiled=True)
    own_normed = lax.dynamic_slice_in_dim(normed, rank * own_rows, own_rows, 0)
    beta = own_live[:, None] * jax.nn.sigmoid(
        jnp.dot(own_normed, w_beta, preferred_element_type=jnp.float32)
    )
    pre = jnp.dot(own_normed, w_decay, preferred_element_type=jnp.float32)
    logdecay = -own_live[:, None] * head_decay_rate * jax.nn.softplus(pre + decay_bias)
    shape = (own, SLOTS, HEADS, HEAD)
    q_own = unit_rows(mine[:, 0].astype(jnp.float32).reshape(shape))
    k_own = unit_rows(mine[:, 1].astype(jnp.float32).reshape(shape))
    v_own = mine[:, 2].astype(jnp.float32).reshape(shape)
    zf = mine[:, 3].astype(jnp.float32).reshape(shape)
    new_state, out = jax.vmap(recur)(
        state,
        q_own,
        k_own,
        v_own,
        beta.reshape(own, SLOTS, HEADS),
        logdecay.reshape(own, SLOTS, HEADS),
    )
    gated = (
        out
        * lax.rsqrt(jnp.mean(out * out, axis=-1, keepdims=True) + EPS)
        * head_gain
        * jax.nn.silu(zf)
    )
    gated = gated.reshape(own_rows, HEADS * HEAD).astype(jnp.bfloat16)
    proj_cols = w_proj.reshape(w_proj.shape[0], -1)
    mixer = jnp.dot(
        lax.all_gather(gated, ("kv", "tp"), axis=0, tiled=True),
        proj_cols,
        preferred_element_type=jnp.float32,
    )
    stream = (hidden.astype(jnp.float32) + mixer[:, None, :]).astype(jnp.bfloat16)
    sf = stream.astype(jnp.float32)
    half_stream = lax.all_gather(stream, "kv", axis=2, tiled=True)[:, 0, :]
    hf = half_stream.astype(jnp.float32)
    squares = lax.psum(jnp.sum(hf * hf, axis=1), "tp")
    gain_half = lax.dynamic_slice_in_dim(ffn_gain, core * half_cols, half_cols)
    fnormed = (hf * lax.rsqrt(squares / D + EPS)[:, None] * gain_half).astype(jnp.bfloat16)
    gate_part = jnp.dot(fnormed, w_gate, preferred_element_type=jnp.float32)
    up_part = jnp.dot(fnormed, w_up, preferred_element_type=jnp.float32)
    gate, upper = (
        lax.psum(gate_part.astype(jnp.bfloat16), "tp").astype(jnp.float32),
        lax.psum(up_part.astype(jnp.bfloat16), "tp").astype(jnp.float32),
    )
    inner = (jax.nn.silu(gate) * upper).astype(jnp.bfloat16)
    partial_down = jnp.dot(inner, w_down, preferred_element_type=jnp.float32)[:, None, :]
    down = lax.psum_scatter(partial_down, "kv", scatter_dimension=2, tiled=True)
    mixed = ((sf + down) * live[:, None, None]).astype(jnp.bfloat16)
    return (mixed, new_state)


def solution(mesh):
    in_specs = (
        P("dp", "tp", "kv"),
        P("dp"),
        P(("dp", "kv", "tp"), None, None, None),
        P(),
        P(None, ("kv", "tp")),
        P(None, ("kv", "tp")),
        P(None, ("kv", "tp")),
        P(None, ("kv", "tp")),
        P(),
        P(),
        P(),
        P(),
        P(),
        P(None, "tp", "kv"),
        P(),
        P("tp", "kv"),
        P("tp", "kv"),
        P("kv", "tp"),
    )
    out_specs = (P("dp", "tp", "kv"), P(("dp", "kv", "tp"), None, None, None))
    return jax.shard_map(local, mesh=mesh, in_specs=in_specs, out_specs=out_specs, check_vma=False)
```

profile of v0, /device:TPU:0, one launch (start us, length us, event | category | flops | bytes accessed | tf_op | source)
XLA Modules:
  0.0 147.9 jit_solution(3823037712257926923)
XLA Ops:
  7.2 15.4 %all_gather.12 = bf16[24,1,2048]{2,0,1:T(8,128)(2,1)S(1)} all-gather(bf16[24,1,512]{2,0,1:T(8,128)(2,1)} %param.18), channel_id=1, replica_groups=mesh['dp'=4,'kv'=4,'tp'=2] {'kv'}, dimensions={2}, use_global_device_ids=true | all-gather | bytes 122880 | tf_op jit(solution)/shard_map/all_gather | solution.py:68
  22.6 1.9 %all_gather.13 = bf16[24,2,2048]{2,0,1:T(8,128)(2,1)S(1)} all-gather(bf16[24,1,2048]{2,0,1:T(8,128)(2,1)S(1)} %all_gather.12), channel_id=1, replica_groups=mesh['dp'=4,'kv'=4,'tp'=2] {'tp'}, dimensions={1}, use_global_device_ids=true | all-gather | bytes 294912 | tf_op jit(solution)/shard_map/all_gather | solution.py:69
  24.8 0.9 multiply_convert_fusion
  26.6 0.9 copy-done.5
  29.1 4.7 %all-to-all-start = ((bf16[24,4,256]{2,1,0:T(4,128)(2,1)}), bf16[24,4,256]{2,1,0:T(4,128)(2,1)S(1)}, u32[]{:S(2)}, u32[]{:S(2)}) async-start(bf16[24,4,256]{2,1,0:T(4,128)(2,1)} %copy.26), calls=%async_computation | async-start | bytes 98304 | tf_op jit(solution)/shard_map/all_to_all | solution.py:81
  36.7 1.0 fusion.19
  37.8 1.9 %all-to-all-done = bf16[24,4,256]{2,1,0:T(4,128)(2,1)S(1)} async-done(((bf16[24,4,256]{2,1,0:T(4,128)(2,1)}), bf16[24,4,256]{2,1,0:T(4,128)(2,1)S(1)}, u32[]{:S(2)}, u32[]{:S(2)}) %all-to-all-start) | async-done | bytes 49184 | tf_op jit(solution)/shard_map/all_to_all | solution.py:81
  40.1 1.1 fusion.30
  41.3 1.2 fusion.28
  42.5 1.2 fusion.26
  43.8 1.4 fusion.24
  45.2 1.5 fusion.22
  46.7 1.1 multiply_add_fusion
  47.8 1.0 copy-done.2
  48.8 1.0 fusion.20
  50.0 14.0 %all-gather = bf16[8,3,2048]{2,1,0:T(4,128)(2,1)S(1)} all-gather(bf16[1,3,2048]{2,1,0:T(4,128)(2,1)S(1)} %fusion.65), channel_id=1, replica_groups=mesh['dp'=4,'kv'=4,'tp'=2] {'kv','tp'}, dimensions={0}, use_global_device_ids=true | all-gather | bytes 110592 | tf_op jit(solution)/shard_map/all_gather | solution.py:110
  64.5 13.2 %all_gather.15 = bf16[24,1,2048]{2,0,1:T(8,128)(2,1)S(1)} all-gather(bf16[24,1,512]{2,0,1:T(8,128)(2,1)S(1)} %fusion.8), channel_id=1, replica_groups=mesh['dp'=4,'kv'=4,'tp'=2] {'kv'}, dimensions={2}, use_global_device_ids=true | all-gather | bytes 122880 | tf_op jit(solution)/shard_map/all_gather | solution.py:116
  77.9 2.6 %psum.21 = f32[24]{0:T(128)S(1)} all-reduce(f32[24]{0:T(128)S(1)} %fusion.50), channel_id=1, replica_groups=mesh['dp'=4,'kv'=4,'tp'=2] {'tp'}, use_global_device_ids=true, to_apply=%region_5.6 | all-reduce | flops 24 | bytes 192 | tf_op jit(solution)/shard_map/psum | solution.py:118
  80.6 6.6 %convolution_convert_fusion.1 = bf16[24,2816]{1,0:T(8,128)(2,1)} fusion(bf16[2048,2816]{1,0:T(8,128)(2,1)} %param.33, bf16[24,1,2048]{2,0,1:T(8,128)(2,1)S(1)} %all_gather.15, f32[2048]{0:T(1024)S(1)} %dynamic_slice.11, f32[24]{0:T(128)S(1)} %add_rsqrt_fusion.3), kind=kOutput, calls=%fused_computation.1 | convolution fusion | flops 277088256 | bytes 11776096 | tf_op jit(solution)/shard_map/dot_general | solution.py:121
  87.2 6.6 %convolution_convert_fusion = bf16[24,2816]{1,0:T(8,128)(2,1)} fusion(bf16[2048,2816]{1,0:T(8,128)(2,1)} %param.34, bf16[24,1,2048]{2,0,1:T(8,128)(2,1)S(1)} %all_gather.15, f32[2048]{0:T(1024)S(1)} %dynamic_slice.11, f32[24]{0:T(128)S(1)} %add_rsqrt_fusion.3), kind=kOutput, calls=%fused_computation | convolution fusion | flops 277088256 | bytes 11776096 | tf_op jit(solution)/shard_map/dot_general | solution.py:122
  93.8 18.0 %all-reduce.3.cloned.1.call-done = (bf16[24,2816]{1,0:T(8,128)(2,1)}, bf16[24,2816]{1,0:T(8,128)(2,1)}) async-done(((bf16[24,2816]{1,0:T(8,128)(2,1)}, bf16[24,2816]{1,0:T(8,128)(2,1)}), (bf16[24,2816]{1,0:T(8,128)(2,1)}, bf16[24,2816]{1,0:T(8,128)(2,1)})) %all-reduce.3.cloned.1.call-update) | async-done | bytes 270352 | tf_op jit(solution)/shard_map/psum | solution.py:125
  111.8 6.7 %convolution_bitcast_fusion = f32[24,1,2048]{2,0,1:T(8,128)} fusion(bf16[2816,2048]{1,0:T(8,128)(2,1)} %param.35, bf16[24,2816]{1,0:T(8,128)(2,1)} %get-tuple-element.2, bf16[24,2816]{1,0:T(8,128)(2,1)} %get-tuple-element.3), kind=kOutput, calls=%fused_computation.2 | convolution fusion | flops 277364736 | bytes 12001280 | tf_op jit(solution)/shard_map/dot_general | solution.py:128
  118.8 20.8 %reduce-scatter.2.cloned.1.call-done = f32[24,1,512]{2,0,1:T(8,128)} async-done(((f32[24,1,2048]{2,0,1:T(8,128)}), f32[24,1,512]{2,0,1:T(8,128)}) %reduce-scatter.2.cloned.1.call-update) | async-done | bytes 49168 | tf_op jit(solution)/shard_map/reduce_scatter | solution.py:129
  139.6 1.5 multiply_convert_fusion.1
  (73 shorter events, 7.3 us)
Async XLA Ops:
  7.2 57.0 %copy-start = (bf16[2048,1,512]{2,0,1:T(8,128)(2,1)S(1)}, bf16[2048,1,512]{2,0,1:T(8,128)(2,1)}, u32[]{:S(2)}) copy-start(bf16[2048,1,512]{2,0,1:T(8,128)(2,1)} %param.31) | copy-start | bytes 6291460
  7.2 18.5 %copy-start.3 = (bf16[4096,256]{1,0:T(8,128)(2,1)S(1)}, bf16[4096,256]{1,0:T(8,128)(2,1)}, u32[]{:S(2)}) copy-start(bf16[4096,256]{1,0:T(8,128)(2,1)} %param.22) | copy-start | bytes 6291460
  24.6 1.6 %copy-start.4 = (bf16[4096,256]{1,0:T(8,128)(2,1)S(1)}, bf16[4096,256]{1,0:T(8,128)(2,1)}, u32[]{:S(2)}) copy-start(bf16[4096,256]{1,0:T(8,128)(2,1)} %param.23) | copy-start | bytes 6291460
  25.7 1.7 %copy-start.5 = (bf16[4096,256]{1,0:T(8,128)(2,1)S(1)}, bf16[4096,256]{1,0:T(8,128)(2,1)}, u32[]{:S(2)}) copy-start(bf16[4096,256]{1,0:T(8,128)(2,1)} %param.24) | copy-start | bytes 6291460
  26.2 1.9 %copy-start.6 = (bf16[4096,256]{1,0:T(8,128)(2,1)S(1)}, bf16[4096,256]{1,0:T(8,128)(2,1)}, u32[]{:S(2)}) copy-start(bf16[4096,256]{1,0:T(8,128)(2,1)} %param.25) | copy-start | bytes 6291460
  27.4 6.4 %copy-start.12 = (s32[8]{0:T(128)S(1)}, s32[8]{0:T(128)}, u32[]{:S(2)}) copy-start(s32[8]{0:T(128)} %param.19) | copy-start | bytes 100
  27.4 8.4 %copy-start.7 = (bf16[4096,16]{0,1:T(8,128)(2,1)S(1)}, bf16[4096,16]{0,1:T(8,128)(2,1)}, u32[]{:S(2)}) copy-start(bf16[4096,16]{0,1:T(8,128)(2,1)} %param.27) | copy-start | bytes 393220
  27.4 8.4 %copy-start.10 = (f32[16]{0:T(128)S(1)}, f32[16]{0:T(128)}, u32[]{:S(2)}) copy-start(f32[16]{0:T(128)} %param.29) | copy-start | bytes 196
  27.4 8.4 %copy-start.11 = (f32[16]{0:T(128)S(1)}, f32[16]{0:T(128)}, u32[]{:S(2)}) copy-start(f32[16]{0:T(128)} %param.28) | copy-start | bytes 196
  27.4 10.3 %copy-start.9 = (f32[4096]{0:T(1024)S(1)}, f32[4096]{0:T(1024)}, u32[]{:S(2)}) copy-start(f32[4096]{0:T(1024)} %param.32) | copy-start | bytes 49156
  28.0 12.1 %copy-start.1 = (f32[1,16,128,128]{3,2,1,0:T(8,128)S(1)}, f32[1,16,128,128]{3,2,1,0:T(8,128)}, u32[]{:S(2)}) copy-start(f32[1,16,128,128]{3,2,1,0:T(8,128)} %param.20) | copy-start | bytes 3145732
  29.1 10.6 %all-to-all-start = ((bf16[24,4,256]{2,1,0:T(4,128)(2,1)}), bf16[24,4,256]{2,1,0:T(4,128)(2,1)S(1)}, u32[]{:S(2)}, u32[]{:S(2)}) async-start(bf16[24,4,256]{2,1,0:T(4,128)(2,1)} %copy.26), calls=%async_computation | async-start | bytes 98304 | tf_op jit(solution)/shard_map/all_to_all | solution.py:81
  33.8 78.0 %all-reduce.3.cloned.1.call-start = ((), (), s32[]{:S(2)}) async-start(), calls=%async_computation.3 | async-start | bytes 540672 | tf_op jit(solution)/shard_map/psum | solution.py:125
  46.7 17.5 %copy-start.8 = (bf16[24,1,512]{2,0,1:T(8,128)(2,1)S(1)}, bf16[24,1,512]{2,0,1:T(8,128)(2,1)}, u32[]{:S(2)}) copy-start(bf16[24,1,512]{2,0,1:T(8,128)(2,1)} %param.18) | copy-start | bytes 73732
  47.8 1.0 copy-start.2
  93.8 45.8 %reduce-scatter.2.cloned.1.call-start = ((), (), s32[]{:S(2)}) async-start(), calls=%async_computation.2 | async-start | bytes 245760 | tf_op jit(solution)/shard_map/reduce_scatter | solution.py:129
  111.8 6.8 %copy-start.13 = (s32[8]{0:T(128)S(1)}, s32[8]{0:T(128)}, u32[]{:S(2)}) copy-start(s32[8]{0:T(128)} %param.19) | copy-start | bytes 100
Sparse Core Ops, SparseCore 0:
  93.9 17.8 all-reduce.2
  118.7 20.8 reduce-scatter.1
where the time goes:
time: 148 us
  blocking collectives  47.2 us (32%)
  waiting for transfers between devices  40.7 us (28%)
  matrix products  30.5 us (21%)
  between operations  14.3 us (10%)
  other arithmetic  6.01 us (4%)
  starting transfers between devices  4.81 us (3%)
  local copies, waits for them, and re-layouts  4.37 us (3%)
    reduce_scatter x1, waiting for transfers between devices, local(): down = lax.psum_scatter(partial_down, 'kv', scatter_dimension=2, tiled=True)  20.8 us
    psum x1, waiting for transfers between devices, local(): lax.psum(up_part.astype(jnp.bfloat16), 'tp').astype(jnp.float32)  18 us
    all_gather x1, blocking collectives, local(): half_rows = lax.all_gather(hidden, 'kv', axis=2, tiled=True)  15.4 us
    all_gather x1, blocking collectives, local(): lax.all_gather(gated, ('kv', 'tp'), axis=0, tiled=True)  14 us
    all_gather x1, blocking collectives, local(): half_stream = lax.all_gather(stream, 'kv', axis=2, tiled=True)[:, 0, :]  13.2 us
    dot_general x1, matrix products, local(): jnp.dot(inner, w_down, preferred_element_type=jnp.float32)[:, None, :]  6.74 us
    dot_general x1, matrix products, local(): gate_part = jnp.dot(fnormed, w_gate, preferred_element_type=jnp.float32)  6.62 us
    dot_general x1, matrix products, local(): up_part = jnp.dot(fnormed, w_up, preferred_element_type=jnp.float32)  6.6 us
  transfers between devices with their start and end apart: 3, of which 3 were waited for; matrix products, arithmetic and copies ran while one was open for 3% of the time, Pallas kernels for 0%

commit v1 on v0

--- a/solution.py
+++ b/solution.py
@@ -1,6 +1,10 @@
+import functools
+
 import jax
 import jax.numpy as jnp
 from jax import lax
+from jax.experimental import pallas as pl
+from jax.experimental.pallas import tpu as pltpu
 from jax.sharding import PartitionSpec as P
 
 D = 4096
@@ -131,6 +135,499 @@
     return (mixed, new_state)
 
 
+def layer_kernel(
+    nk,
+    hidden,
+    lengths,
+    state_hbm,
+    attn_gain,
+    wq_hbm,
+    wk_hbm,
+    wv_hbm,
+    wz_hbm,
+    wb_hbm,
+    wd_hbm,
+    rate,
+    bias,
+    head_gain,
+    wp_hbm,
+    ffn_gain,
+    wg_hbm,
+    wu_hbm,
+    wdn_hbm,
+    mixed,
+    state_out,
+    w_all,
+    w_p,
+    w_g,
+    w_u,
+    w_dn,
+    w_bd,
+    st,
+    hx,
+    acc,
+    blocks,
+    scale,
+    px,
+    rx,
+    flat,
+    qk,
+    qkt,
+    outs,
+    gx,
+    rg,
+    flat2,
+    sx,
+    acc_g,
+    acc_u,
+    xs,
+    rs,
+    sq,
+    rsq,
+    dx,
+    rd,
+    w_sem,
+    h_send,
+    h_recv,
+    p_send,
+    p_recv,
+    g_send,
+    g_recv,
+    s_send,
+    s_recv,
+    x_send,
+    x_recv,
+    d_send,
+    d_recv,
+):
+    f32, bf16 = jnp.float32, jnp.bfloat16
+    c = lax.axis_index("kv")
+    t = lax.axis_index("tp")
+    me = c * 2 + t
+    group = 2 * nk
+    rows, piece = hidden.shape
+    cols = w_p.shape[0] // group
+    seqs = rows // SLOTS
+    width = group * piece
+    turn = 1 - 2 * (c // max(nk // 2, 1))
+
+    def near(i):
+        return lax.rem(c + turn * i + nk, nk)
+
+    def send(src, dst, ssem, rsem, kv, tp):
+        copy = pltpu.make_async_remote_copy(
+            src_ref=src,
+            dst_ref=dst,
+            send_sem=ssem,
+            recv_sem=rsem,
+            device_id={"kv": kv, "tp": tp},
+            device_id_type=pl.DeviceIdType.MESH,
+        )
+        copy.start()
+        return copy
+
+    def arrived(ref, ssem, rsem):
+        pltpu.make_async_remote_copy(
+            src_ref=ref,
+            dst_ref=ref,
+            send_sem=ssem,
+            recv_sem=rsem,
+            device_id={"kv": c, "tp": 1 - t},
+            device_id_type=pl.DeviceIdType.MESH,
+        ).wait_recv()
+
+    loads = []
+
+    def load(src, dst):
+        copy = pltpu.make_async_copy(src, dst, w_sem.at[len(loads)])
+        copy.start()
+        loads.append(copy)
+        return copy
+
+    own_off = pl.multiple_of((t * nk + c) * piece, piece)
+    load_b = load(wb_hbm.at[:, pl.ds(own_off, piece)], w_bd.at[0:HEADS, :])
+    load_d = load(wd_hbm.at[:, pl.ds(own_off, piece)], w_bd.at[HEADS : 2 * HEADS, :])
+    w_bd[2 * HEADS :, :] = jnp.zeros((HEAD - 2 * HEADS, piece), bf16)
+    load_proj = [load(w, w_all.at[j]) for j, w in enumerate((wq_hbm, wk_hbm, wv_hbm, wz_hbm))]
+    load_state = load(state_hbm, st)
+    load_p = load(wp_hbm, w_p)
+    load_gu = [
+        [load(a.at[pl.ds(near(i) * piece, piece), :], b.at[pl.ds(near(i) * piece, piece), :])
+         for a, b in ((wg_hbm, w_g), (wu_hbm, w_u))]
+        for i in range(nk)
+    ]
+    part = w_dn.shape[0] // 4
+    load_dn = [
+        load(wdn_hbm.at[pl.ds(i * part, part), :], w_dn.at[pl.ds(i * part, part), :])
+        for i in range(4)
+    ]
+
+    barrier = pltpu.get_barrier_semaphore()
+    others = [(i, j) for i in range(nk) for j in range(2) if i or j]
+    for i, j in others:
+        pl.semaphore_signal(
+            barrier,
+            inc=1,
+            device_id={"kv": near(i), "tp": lax.rem(t + j, 2)},
+            device_id_type=pl.DeviceIdType.MESH,
+        )
+    pl.semaphore_wait(barrier, len(others))
+
+    sends = []
+    own_slot = t * nk + c
+    for i in range(1, nk):
+        sends.append(
+            send(hidden, hx.at[own_slot], h_send.at[i], h_recv.at[own_slot], near(i), t)
+        )
+    sends.append(send(hidden, hx.at[own_slot], h_send.at[0], h_recv.at[own_slot], c, 1 - t))
+
+    def scaled(x, gain_ref, slot):
+        gain = gain_ref[:, pl.ds(pl.multiple_of(slot * piece, piece), piece)]
+        return (x * gain).astype(bf16)
+
+    def proj(x, slot):
+        return [
+            jnp.dot(
+                x,
+                w_all[j, pl.ds(pl.multiple_of(slot * piece, piece), piece), :],
+                preferred_element_type=f32,
+            )
+            for j in range(4)
+        ]
+
+    hf = hidden[...].astype(f32)
+    xg = scaled(hf, attn_gain, own_slot)
+    load_b.wait()
+    load_d.wait()
+    pbd = lax.dot_general(xg, w_bd[...], (((1,), (1,)), ((), ())), preferred_element_type=f32)
+    for copy in load_proj:
+        copy.wait()
+    for j, value in enumerate(proj(xg, own_slot)):
+        acc[:, j * cols : (j + 1) * cols] = value
+    squares = jnp.sum(hf * hf, axis=1, keepdims=True)
+
+    def slot_step(slot, squares):
+        xf = hx[slot].astype(f32)
+        for j, value in enumerate(proj(scaled(xf, attn_gain, slot), slot)):
+            acc[:, j * cols : (j + 1) * cols] += value
+        return squares + jnp.sum(xf * xf, axis=1, keepdims=True)
+
+    for i in range(1, nk):
+        slot = t * nk + near(i)
+        arrived(hx.at[slot], h_send.at[0], h_recv.at[slot])
+        sends.append(
+            send(hx.at[slot], hx.at[slot], h_send.at[nk - 1 + i], h_recv.at[slot], c, 1 - t)
+        )
+    squares = lax.fori_loop(
+        1, nk, lambda i, total: slot_step(t * nk + near(i), total), squares
+    )
+
+    def partner_step(i, total):
+        slot = (1 - t) * nk + near(i)
+        arrived(hx.at[slot], h_send.at[0], h_recv.at[slot])
+        return slot_step(slot, total)
+
+    squares = lax.fori_loop(0, nk, partner_step, squares)
+    rms = lax.rsqrt(squares / width + EPS)
+    scale[...] = jnp.broadcast_to(rms, (rows, HEAD))
+    per = 4 * cols // HEAD
+    for j in range(per):
+        blocks[pl.ds(j, rows, stride=per), :] = acc[:, j * HEAD : (j + 1) * HEAD] * rms
+    high = pbd.astype(bf16).astype(f32)
+    low = pbd - high
+    zero = jnp.zeros((2, HEAD), f32)
+    span = SLOTS * per
+    for g in range(group):
+        at = slice(g * SLOTS, (g + 1) * SLOTS)
+        px[g, 0:span, :] = blocks[g * span : (g + 1) * span, :].astype(bf16)
+        px[g, span : span + 8, :] = jnp.concatenate([high[at], low[at], zero], axis=0).astype(bf16)
+    for i, j in others:
+        kv, tp = near(i), lax.rem(t + j, 2)
+        sends.append(
+            send(px.at[kv * 2 + tp], rx.at[me], p_send.at[i * 2 + j], p_recv.at[me], kv, tp)
+        )
+    rx[me] = px[me]
+    tall = span + 8
+
+    own_len = lengths[me]
+    own_rms = [scale[pl.ds(me * SLOTS + s, 1), :] for s in range(SLOTS)]
+    load_state.wait()
+    for i, j in others:
+        src = near(i) * 2 + lax.rem(t + j, 2)
+        arrived(rx.at[src], p_send.at[0], p_recv.at[src])
+    for g in range(group):
+        flat[g * tall : (g + 1) * tall, :] = rx[g].astype(f32)
+    hh = cols // HEAD
+
+    def tile(s, p, h):
+        return flat[pl.ds(s * per + p * hh + h, group, stride=tall), :]
+
+    def unit(x):
+        return x * lax.rsqrt(jnp.sum(x * x, axis=1, keepdims=True) + EPS)
+
+    qk[...] = jnp.zeros_like(qk)
+    for s in range(SLOTS):
+        for h in range(hh):
+            at = (s * hh + h) * group
+            qk[at : at + group, :] = unit(tile(s, 0, h))
+            at += SLOTS * HEADS
+            qk[at : at + group, :] = unit(tile(s, 1, h))
+    qkt[...] = qk[...].T
+    betas, decays = [], []
+    for s in range(SLOTS):
+        pre = jnp.sum(
+            flat[pl.ds(span + s, group, stride=tall), :]
+            + flat[pl.ds(span + SLOTS + s, group, stride=tall), :],
+            axis=0,
+            keepdims=True,
+        ) * own_rms[s]
+        live = jnp.where(s < own_len, 1.0, 0.0).astype(f32)
+        betas.append(live * jax.nn.sigmoid(pre[:, :HEADS]))
+        arg = pre[:, HEADS : 2 * HEADS] + bias[...]
+        soft = jnp.maximum(arg, 0.0) + jnp.log1p(jnp.exp(-jnp.abs(arg)))
+        decays.append(jnp.exp(-live * rate[...] * soft))
+    inv = HEAD**-0.5
+    state_copies = []
+    for src in range(group):
+        for h in range(hh):
+            n = src * hh + h
+            S = st[n]
+            for s in range(SLOTS):
+                col = (s * hh + h) * group + src
+                kc = qkt[:, col + SLOTS * HEADS : col + SLOTS * HEADS + 1]
+                qc = qkt[:, col : col + 1]
+                v = flat[src * tall + s * per + 2 * hh + h : src * tall + s * per + 2 * hh + h + 1, :]
+                S = S * decays[s][:, n : n + 1]
+                recalled = jnp.sum(S * kc, axis=0, keepdims=True)
+                change = betas[s][:, n : n + 1] * (v - recalled)
+                S = S + kc * change
+                outs[col : col + 1, :] = jnp.sum(S * qc, axis=0, keepdims=True) * inv
+            st[n] = S
+    for s in range(SLOTS):
+        for h in range(hh):
+            at = (s * hh + h) * group
+            o = outs[at : at + group, :]
+            z = tile(s, 3, h)
+            gated = (
+                o
+                * lax.rsqrt(jnp.mean(o * o, axis=1, keepdims=True) + EPS)
+                * head_gain[...]
+                * (z * jax.nn.sigmoid(z))
+            )
+            outs[at : at + group, :] = gated
+    gx[...] = outs[...].astype(bf16)
+    for i, j in others:
+        kv, tp = near(i), lax.rem(t + j, 2)
+        sends.append(send(gx, rg.at[me], g_send.at[i * 2 + j], g_recv.at[me], kv, tp))
+    rg[me] = gx[...]
+    state_copy = pltpu.make_async_copy(st, state_out, w_sem.at[len(loads)])
+    state_copy.start()
+    load_p.wait()
+    for i, j in others:
+        src = near(i) * 2 + lax.rem(t + j, 2)
+        arrived(rg.at[src], g_send.at[0], g_recv.at[src])
+    for g in range(group):
+        flat2[g * SLOTS * HEADS : (g + 1) * SLOTS * HEADS, :] = rg[g].astype(f32)
+    gall = jnp.concatenate(
+        [
+            flat2[pl.ds((n % hh) * group + n // hh, rows, stride=HEADS), :].astype(bf16)
+            for n in range(HEADS)
+        ],
+        axis=1,
+    )
+    mixer = jnp.dot(gall, w_p[...], preferred_element_type=f32)
+    sx[c] = (hf + mixer).astype(bf16)
+    for i in range(1, nk):
+        sends.append(send(sx.at[c], sx.at[c], s_send.at[i], s_recv.at[c], near(i), t))
+
+    acc_g[...] = jnp.zeros_like(acc_g)
+    acc_u[...] = jnp.zeros_like(acc_u)
+    for i in range(nk):
+        for copy in load_gu[i]:
+            copy.wait()
+
+    def ffn_step(i, total):
+        slot = near(i)
+
+        @pl.when(i > 0)
+        def _():
+            arrived(sx.at[slot], s_send.at[0], s_recv.at[slot])
+
+        xf = sx[slot].astype(f32)
+        x = scaled(xf, ffn_gain, t * nk + slot)
+        at = pl.ds(pl.multiple_of(slot * piece, piece), piece)
+        acc_g[...] += jnp.dot(x, w_g[at, :], preferred_element_type=f32)
+        acc_u[...] += jnp.dot(x, w_u[at, :], preferred_element_type=f32)
+        return total + jnp.sum(xf * xf, axis=1, keepdims=True)
+
+    half = lax.fori_loop(0, nk, ffn_step, jnp.zeros((rows, 1), f32))
+    sq[...] = jnp.broadcast_to(half, (rows, HEAD))
+    xs[0] = acc_g[...].astype(bf16)
+    xs[1] = acc_u[...].astype(bf16)
+    x0 = send(sq, rsq, x_send.at[0], x_recv.at[0], c, 1 - t)
+    x1 = send(xs, rs, x_send.at[1], x_recv.at[1], c, 1 - t)
+    sends += [x0, x1]
+    for copy in load_dn:
+        copy.wait()
+    x0.wait_recv()
+    x1.wait_recv()
+    fr = lax.rsqrt((half + rsq[:, 0:1]) / width + EPS)
+    gate = (acc_g[...] + rs[0].astype(f32)) * fr
+    upper = (acc_u[...] + rs[1].astype(f32)) * fr
+    inner = (gate * jax.nn.sigmoid(gate) * upper).astype(bf16)
+    xs_inner = inner
+
+    def down(slot):
+        at = pl.ds(pl.multiple_of(slot * piece, piece), piece)
+        return jnp.dot(xs_inner, w_dn[:, at], preferred_element_type=f32)
+
+    for i in range(nk - 1, 0, -1):
+        slot = near(i)
+        dx[i] = down(slot).astype(bf16)
+        sends.append(send(dx.at[i], rd.at[c], d_send.at[i], d_recv.at[c], slot, t))
+    total = sx[c].astype(f32) + down(c)
+    row = lax.broadcasted_iota(jnp.int32, (rows, piece), 0)
+    live = jnp.zeros((rows, piece), f32)
+    for n in range(seqs):
+        hit = (row >= n * SLOTS) & (row < n * SLOTS + lengths[n])
+        live = jnp.where(hit, 1.0, live)
+    for i in range(1, nk):
+        slot = near(i)
+        arrived(rd.at[slot], d_send.at[0], d_recv.at[slot])
+        total = total + rd[slot].astype(f32)
+    mixed[...] = (total * live).astype(bf16)
+    for copy in sends:
+        copy.wait_send()
+    state_copy.wait()
+
+
+def fused(
+    nk,
+    hidden,
+    lengths,
+    state,
+    attn_gain,
+    w_query,
+    w_key,
+    w_value,
+    w_outgate,
+    w_beta,
+    w_decay,
+    head_decay_rate,
+    decay_bias,
+    head_gain,
+    w_proj,
+    ffn_gain,
+    w_gate,
+    w_up,
+    w_down,
+):
+    f32, bf16 = jnp.float32, jnp.bfloat16
+    rows, _, piece = hidden.shape
+    group = 2 * nk
+    depth, cols = w_query.shape
+    hd = w_proj.shape[0]
+    half, ff = w_gate.shape
+    per = 4 * cols // HEAD
+    tall = SLOTS * per + 8
+    vmem = pl.BlockSpec(memory_space=pltpu.VMEM)
+    smem = pl.BlockSpec(memory_space=pltpu.SMEM)
+    hbm = pl.BlockSpec(memory_space=pl.ANY)
+    dma = pltpu.SemaphoreType.DMA
+    mixed, new_state = pl.pallas_call(
+        functools.partial(layer_kernel, nk),
+        out_shape=(
+            jax.ShapeDtypeStruct((rows, piece), bf16),
+            jax.ShapeDtypeStruct(state.shape[1:], f32),
+        ),
+        in_specs=[vmem, smem, hbm, vmem] + [hbm] * 6 + [vmem] * 3 + [hbm, vmem] + [hbm] * 3,
+        out_specs=(vmem, hbm),
+        scratch_shapes=[
+            pltpu.VMEM((4, depth, cols), bf16),
+            pltpu.VMEM((hd, piece), bf16),
+            pltpu.VMEM((half, ff), bf16),
+            pltpu.VMEM((half, ff), bf16),
+            pltpu.VMEM(w_down.shape, bf16),
+            pltpu.VMEM((HEAD, piece), bf16),
+            pltpu.VMEM(state.shape[1:], f32),
+            pltpu.VMEM((group, rows, piece), bf16),
+            pltpu.VMEM((rows, 4 * cols), f32),
+            pltpu.VMEM((rows * per, HEAD), f32),
+            pltpu.VMEM((rows, HEAD), f32),
+            pltpu.VMEM((group, tall, HEAD), bf16),
+            pltpu.VMEM((group, tall, HEAD), bf16),
+            pltpu.VMEM((group * tall, HEAD), f32),
+            pltpu.VMEM((HEAD, HEAD), f32),
+            pltpu.VMEM((HEAD, HEAD), f32),
+            pltpu.VMEM((SLOTS * HEADS, HEAD), f32),
+            pltpu.VMEM((SLOTS * HEADS, HEAD), bf16),
+            pltpu.VMEM((group, SLOTS * HEADS, HEAD), bf16),
+            pltpu.VMEM((group * SLOTS * HEADS, HEAD), f32),
+            pltpu.VMEM((nk, rows, piece), bf16),
+            pltpu.VMEM((rows, ff), f32),
+            pltpu.VMEM((rows, ff), f32),
+            pltpu.VMEM((2, rows, ff), bf16),
+            pltpu.VMEM((2, rows, ff), bf16),
+            pltpu.VMEM((rows, HEAD), f32),
+            pltpu.VMEM((rows, HEAD), f32),
+            pltpu.VMEM((nk, rows, piece), bf16),
+            pltpu.VMEM((nk, rows, piece), bf16),
+            dma((13 + 2 * nk,)),
+            dma((group,)),
+            dma((group,)),
+            dma((group,)),
+            dma((group,)),
+            dma((group,)),
+            dma((group,)),
+            dma((nk,)),
+            dma((nk,)),
+            dma((2,)),
+            dma((2,)),
+            dma((nk,)),
+            dma((nk,)),
+        ],
+        compiler_params=pltpu.CompilerParams(
+            collective_id=0, has_side_effects=True, vmem_limit_bytes=62 * 2**20
+        ),
+        name="layer",
+    )(
+        hidden.reshape(rows, piece),
+        lengths,
+        state.reshape(state.shape[1:]),
+        attn_gain.reshape(1, -1),
+        w_query,
+        w_key,
+        w_value,
+        w_outgate,
+        w_beta.T,
+        w_decay.T,
+        head_decay_rate.reshape(1, -1),
+        decay_bias.reshape(1, -1),
+        head_gain.reshape(1, -1),
+        w_proj.reshape(hd, piece),
+        ffn_gain.reshape(1, -1),
+        w_gate,
+        w_up,
+        w_down,
+    )
+    return mixed.reshape(hidden.shape), new_state.reshape(state.shape)
+
+
+def dispatch(nk, nt, hidden, lengths, state, *rest):
+    piece, cols = hidden.shape[2], rest[1].shape[1]
+    fits = (
+        nt == 2
+        and nk == 4
+        and state.shape[0] == 1
+        and hidden.shape[0] % 8 == 0
+        and piece % HEAD == 0
+        and cols % HEAD == 0
+        and rest[-3].shape[1] % HEAD == 0
+    )
+    plan = functools.partial(fused, nk) if fits else local
+    return plan(hidden, lengths, state, *rest)
+
+
 def solution(mesh):
     in_specs = (
         P("dp", "tp", "kv"),
@@ -153,4 +650,5 @@
         P("kv", "tp"),
     )
     out_specs = (P("dp", "tp", "kv"), P(("dp", "kv", "tp"), None, None, None))
-    return jax.shard_map(local, mesh=mesh, in_specs=in_specs, out_specs=out_specs, check_vma=False)
+    plan = functools.partial(dispatch, mesh.shape["kv"], mesh.shape["tp"])
+    return jax.shard_map(plan, mesh=mesh, in_specs=in_specs, out_specs=out_specs, check_vma=False)

time: 148 us -> 40.6 us (0.27)
  blocking collectives: 47.2 us -> 0 us
  waiting for transfers between devices: 40.7 us -> 0 us
  Pallas kernels: 0 us -> 35.7 us
  matrix products: 30.5 us -> 0 us
  between operations: 14.3 us -> 0.65 us
  other arithmetic: 6.01 us -> 0 us
  starting transfers between devices: 4.81 us -> 0 us
    all_gather x4 -> x0, blocking collectives: 44.6 us -> none  [the longest x1 15.4 us: local(): half_rows = lax.all_gather(hidden, 'kv', axis=2, tiled=True)]
    pallas_call x0 -> x1, Pallas kernels: none -> 35.7 us  [fused(): pl.pallas_call(functools.partial(layer_kernel, nk), out_shape=(jax.ShapeD...]
    dot_general x16 -> x0, matrix products: 30.5 us -> none  [the longest x1 6.74 us: local(): jnp.dot(inner, w_down, preferred_element_type=jnp.float32)[:, None, :]]
    reduce_scatter x1 -> x0, waiting for transfers between devices: 20.8 us -> none  [local(): down = lax.psum_scatter(partial_down, 'kv', scatter_dimension=2, tiled=True)]
    psum x1 -> x0, waiting for transfers between devices: 18 us -> none  [local(): lax.psum(up_part.astype(jnp.bfloat16), 'tp').astype(jnp.float32)]
    all_to_all x1 -> x0, starting transfers between devices: 4.73 us -> none  [local(): lax.all_to_all(projected, ('kv', 'tp'), split_axis=0, concat_axis=2, tile...]
    convert_element_type x5 -> x0, other arithmetic: 3.2 us -> none  [the longest x1 1.48 us: local(): mixed = ((sf + down) * live[:, None, None]).astype(jnp.bfloat16)]
    psum x1 -> x0, blocking collectives: 2.64 us -> none  [local(): squares = lax.psum(jnp.sum(hf * hf, axis=1), 'tp')]
  transfers between devices with their start and end apart: 3 -> 0, of which waited for: 3 -> 0; matrix products, arithmetic and copies ran while one was open for 3% -> 0% of each run, Pallas kernels for 0% -> 0%
where the time goes in v1:
time: 40.6 us; the launch traced here: 40 us
  Pallas kernels  35.7 us (88%)
  local copies, waits for them, and re-layouts  3.64 us (9%)
  between operations  0.65 us (2%)
    pallas_call x1, Pallas kernels, fused(): pl.pallas_call(functools.partial(layer_kernel, nk), out_shape=(jax.ShapeD...  35.7 us
    unnamed x2, local copies, waits for them, and re-layouts  3.64 us

profile of v1, /device:TPU:0, one launch (start us, length us, event | category | flops | bytes accessed | tf_op | source)
XLA Modules:
  0.0 40.0 jit_solution(15917344048468691060)
XLA Ops:
  0.6 35.7 %layer.1 = (bf16[24,512]{1,0:T(8,128)(2,1)}, f32[16,128,128]{2,1,0:T(8,128)}) custom-call(bf16[24,512]{1,0:T(8,128)(2,1)} %bitcast.18, s32[8]{0:T(128)} %lengths.1, f32[16,128,128]{2,1,0:T(8,128)} %bitcast.14, f32[1,4096]{1,0:T(1,128)} %bitcast.19, bf16[4096,256]{1,0:T(8,128)(2,1)} %wq_hbm.1, bf16[4096,256]{1,0:T(8,128)(2,1)} %wk_hbm.1, ...), custom_call_target="tpu_custom_call" | custom-call | tf_op jit(solution)/shard_map/layer/pallas_call | solution.py:537
  36.3 1.3 %copy.22 = bf16[24,1,512]{2,0,1:T(8,128)(2,1)} copy(bf16[24,1,512]{2,0,1:T(8,128)(2,1)} %bitcast.17) | data formatting | bytes 49152
  37.7 2.3 %copy.23 = f32[1,16,128,128]{3,2,1,0:T(8,128)} copy(f32[1,16,128,128]{3,2,1,0:T(8,128)} %bitcast.13) | data formatting | bytes 2097152

commit v2 on v1

--- a/solution.py
+++ b/solution.py
@@ -138,20 +138,20 @@
 def layer_kernel(
     nk,
     hidden,
-    lengths,
+    lengths_hbm,
     state_hbm,
-    attn_gain,
+    attn_gain_hbm,
     wq_hbm,
     wk_hbm,
     wv_hbm,
     wz_hbm,
     wb_hbm,
     wd_hbm,
-    rate,
-    bias,
-    head_gain,
+    rate_hbm,
+    bias_hbm,
+    head_gain_hbm,
     wp_hbm,
-    ffn_gain,
+    ffn_gain_hbm,
     wg_hbm,
     wu_hbm,
     wdn_hbm,
@@ -186,6 +186,12 @@
     rsq,
     dx,
     rd,
+    lengths,
+    attn_gain,
+    ffn_gain,
+    rate,
+    bias,
+    head_gain,
     w_sem,
     h_send,
     h_recv,
@@ -236,6 +242,15 @@
             device_id_type=pl.DeviceIdType.MESH,
         ).wait_recv()
 
+    barrier = pltpu.get_barrier_semaphore()
+    others = [(i, j) for i in reversed(range(nk)) for j in range(2) if i or j]
+    for i, j in others:
+        pl.semaphore_signal(
+            barrier,
+            inc=1,
+            device_id={"kv": near(i), "tp": lax.rem(t + j, 2)},
+            device_id_type=pl.DeviceIdType.MESH,
+        )
     loads = []
 
     def load(src, dst):
@@ -244,7 +259,20 @@
         loads.append(copy)
         return copy
 
-    own_off = pl.multiple_of((t * nk + c) * piece, piece)
+    own_slot = t * nk + c
+    own_off = pl.multiple_of(own_slot * piece, piece)
+    load_hidden = load(hidden, hx.at[own_slot])
+    load_small = [
+        load(a, b)
+        for a, b in (
+            (attn_gain_hbm, attn_gain),
+            (lengths_hbm, lengths),
+            (ffn_gain_hbm, ffn_gain),
+            (rate_hbm, rate),
+            (bias_hbm, bias),
+            (head_gain_hbm, head_gain),
+        )
+    ]
     load_b = load(wb_hbm.at[:, pl.ds(own_off, piece)], w_bd.at[0:HEADS, :])
     load_d = load(wd_hbm.at[:, pl.ds(own_off, piece)], w_bd.at[HEADS : 2 * HEADS, :])
     w_bd[2 * HEADS :, :] = jnp.zeros((HEAD - 2 * HEADS, piece), bf16)
@@ -262,24 +290,14 @@
         for i in range(4)
     ]
 
-    barrier = pltpu.get_barrier_semaphore()
-    others = [(i, j) for i in range(nk) for j in range(2) if i or j]
-    for i, j in others:
-        pl.semaphore_signal(
-            barrier,
-            inc=1,
-            device_id={"kv": near(i), "tp": lax.rem(t + j, 2)},
-            device_id_type=pl.DeviceIdType.MESH,
-        )
+    sends = []
+    load_hidden.wait()
     pl.semaphore_wait(barrier, len(others))
 
-    sends = []
-    own_slot = t * nk + c
-    for i in range(1, nk):
-        sends.append(
-            send(hidden, hx.at[own_slot], h_send.at[i], h_recv.at[own_slot], near(i), t)
-        )
-    sends.append(send(hidden, hx.at[own_slot], h_send.at[0], h_recv.at[own_slot], c, 1 - t))
+    mine = hx.at[own_slot]
+    for i in reversed(range(1, nk)):
+        sends.append(send(mine, mine, h_send.at[i], h_recv.at[own_slot], near(i), t))
+    sends.append(send(mine, mine, h_send.at[0], h_recv.at[own_slot], c, 1 - t))
 
     def scaled(x, gain_ref, slot):
         gain = gain_ref[:, pl.ds(pl.multiple_of(slot * piece, piece), piece)]
@@ -295,7 +313,9 @@
             for j in range(4)
         ]
 
-    hf = hidden[...].astype(f32)
+    for copy in load_small:
+        copy.wait()
+    hf = hx[own_slot].astype(f32)
     xg = scaled(hf, attn_gain, own_slot)
     load_b.wait()
     load_d.wait()
@@ -318,9 +338,7 @@
         sends.append(
             send(hx.at[slot], hx.at[slot], h_send.at[nk - 1 + i], h_recv.at[slot], c, 1 - t)
         )
-    squares = lax.fori_loop(
-        1, nk, lambda i, total: slot_step(t * nk + near(i), total), squares
-    )
+        squares = slot_step(slot, squares)
 
     def partner_step(i, total):
         slot = (1 - t) * nk + near(i)
@@ -402,7 +420,7 @@
                 change = betas[s][:, n : n + 1] * (v - recalled)
                 S = S + kc * change
                 outs[col : col + 1, :] = jnp.sum(S * qc, axis=0, keepdims=True) * inv
-            st[n] = S
+            state_out[n] = S
     for s in range(SLOTS):
         for h in range(hh):
             at = (s * hh + h) * group
@@ -420,8 +438,6 @@
         kv, tp = near(i), lax.rem(t + j, 2)
         sends.append(send(gx, rg.at[me], g_send.at[i * 2 + j], g_recv.at[me], kv, tp))
     rg[me] = gx[...]
-    state_copy = pltpu.make_async_copy(st, state_out, w_sem.at[len(loads)])
-    state_copy.start()
     load_p.wait()
     for i, j in others:
         src = near(i) * 2 + lax.rem(t + j, 2)
@@ -437,7 +453,7 @@
     )
     mixer = jnp.dot(gall, w_p[...], preferred_element_type=f32)
     sx[c] = (hf + mixer).astype(bf16)
-    for i in range(1, nk):
+    for i in reversed(range(1, nk)):
         sends.append(send(sx.at[c], sx.at[c], s_send.at[i], s_recv.at[c], near(i), t))
 
     acc_g[...] = jnp.zeros_like(acc_g)
@@ -498,7 +514,16 @@
     mixed[...] = (total * live).astype(bf16)
     for copy in sends:
         copy.wait_send()
-    state_copy.wait()
+
+
+def write_kernel(a, b, a_out, b_out, sem):
+    copies = [
+        pltpu.make_async_copy(x, y, sem.at[n]) for n, (x, y) in enumerate(((b, b_out), (a, a_out)))
+    ]
+    for copy in copies:
+        copy.start()
+    for copy in copies:
+        copy.wait()
 
 
 def fused(
@@ -531,17 +556,16 @@
     per = 4 * cols // HEAD
     tall = SLOTS * per + 8
     vmem = pl.BlockSpec(memory_space=pltpu.VMEM)
-    smem = pl.BlockSpec(memory_space=pltpu.SMEM)
     hbm = pl.BlockSpec(memory_space=pl.ANY)
     dma = pltpu.SemaphoreType.DMA
     mixed, new_state = pl.pallas_call(
         functools.partial(layer_kernel, nk),
         out_shape=(
-            jax.ShapeDtypeStruct((rows, piece), bf16),
-            jax.ShapeDtypeStruct(state.shape[1:], f32),
+            pltpu.VMEM((rows, piece), bf16),
+            pltpu.VMEM(state.shape[1:], f32),
         ),
-        in_specs=[vmem, smem, hbm, vmem] + [hbm] * 6 + [vmem] * 3 + [hbm, vmem] + [hbm] * 3,
-        out_specs=(vmem, hbm),
+        in_specs=[hbm] * 18,
+        out_specs=(vmem, vmem),
         scratch_shapes=[
             pltpu.VMEM((4, depth, cols), bf16),
             pltpu.VMEM((hd, piece), bf16),
@@ -572,7 +596,13 @@
             pltpu.VMEM((rows, HEAD), f32),
             pltpu.VMEM((nk, rows, piece), bf16),
             pltpu.VMEM((nk, rows, piece), bf16),
-            dma((13 + 2 * nk,)),
+            pltpu.SMEM(lengths.shape, jnp.int32),
+            pltpu.VMEM((1, 2 * half), f32),
+            pltpu.VMEM((1, 2 * half), f32),
+            pltpu.VMEM((1, HEADS), f32),
+            pltpu.VMEM((1, HEADS), f32),
+            pltpu.VMEM((1, HEAD), f32),
+            dma((20 + 2 * nk,)),
             dma((group,)),
             dma((group,)),
             dma((group,)),
@@ -587,7 +617,7 @@
             dma((nk,)),
         ],
         compiler_params=pltpu.CompilerParams(
-            collective_id=0, has_side_effects=True, vmem_limit_bytes=62 * 2**20
+            collective_id=0, has_side_effects=True, vmem_limit_bytes=60 * 2**20
         ),
         name="layer",
     )(
@@ -610,6 +640,17 @@
         w_up,
         w_down,
     )
+    mixed, new_state = pl.pallas_call(
+        write_kernel,
+        out_shape=(
+            jax.ShapeDtypeStruct((rows, piece), bf16),
+            jax.ShapeDtypeStruct(state.shape[1:], f32),
+        ),
+        in_specs=[vmem, vmem],
+        out_specs=(hbm, hbm),
+        scratch_shapes=[dma((2,))],
+        name="write",
+    )(*[pltpu.with_memory_space_constraint(x, pltpu.VMEM) for x in (mixed, new_state)])
     return mixed.reshape(hidden.shape), new_state.reshape(state.shape)
 
 

time: 40.6 us -> 35.4 us (0.87)
  local copies, waits for them, and re-layouts: 3.64 us -> 0 us
  Pallas kernels: 35.7 us -> 34.5 us
    unnamed x2 -> x0, local copies, waits for them, and re-layouts: 3.64 us -> none
    pallas_call x1 -> x2, Pallas kernels: 35.7 us -> 34.5 us  [the longest x1 33.5 us: fused(): pl.pallas_call(functools.partial(layer_kernel, nk), out_shape=(pltpu.VMEM...]
where the time goes in v2:
time: 35.4 us; the launch traced here: 35.1 us
  Pallas kernels  34.5 us (97%)
  between operations  0.65 us (2%)
    pallas_call x1, Pallas kernels, fused(): pl.pallas_call(functools.partial(layer_kernel, nk), out_shape=(pltpu.VMEM...  33.5 us
    pallas_call x1, Pallas kernels, fused(): pl.pallas_call(write_kernel, out_shape=(jax.ShapeDtypeStruct((rows, piece...  0.99 us

profile of v2, /device:TPU:0, one launch (start us, length us, event | category | flops | bytes accessed | tf_op | source)
XLA Modules:
  0.0 35.1 jit_solution(15225682685902853378)
XLA Ops:
  0.6 33.5 %layer.1 = (bf16[24,512]{1,0:T(8,128)(2,1)S(1)}, f32[16,128,128]{2,1,0:T(8,128)S(1)}) custom-call(bf16[24,512]{1,0:T(8,128)(2,1)} %bitcast.16, s32[8]{0:T(128)} %lengths_hbm.1, f32[16,128,128]{2,1,0:T(8,128)} %bitcast.13, f32[1,4096]{1,0:T(1,128)} %bitcast.17, bf16[4096,256]{1,0:T(8,128)(2,1)} %wq_hbm.1, bf16[4096,256]{1,0:T(8,128)(2,1)} %wk_hbm.1, ...), custom_call_target="tpu_custom_call" | custom-call | tf_op jit(solution)/shard_map/layer/pallas_call | solution.py:561
  34.1 1.0 %write.1 = (bf16[24,512]{1,0:T(8,128)(2,1)}, f32[16,128,128]{2,1,0:T(8,128)}) custom-call(bf16[24,512]{1,0:T(8,128)(2,1)S(1)} %get-tuple-element.6.a, f32[16,128,128]{2,1,0:T(8,128)S(1)} %get-tuple-element.7.b), custom_call_target="tpu_custom_call" | custom-call | tf_op jit(solution)/shard_map/write/pallas_call | solution.py:643

commit v3 on v2

--- a/solution.py
+++ b/solution.py
@@ -390,8 +390,6 @@
             qk[at : at + group, :] = unit(tile(s, 0, h))
             at += SLOTS * HEADS
             qk[at : at + group, :] = unit(tile(s, 1, h))
-    qkt[...] = qk[...].T
-    betas, decays = [], []
     for s in range(SLOTS):
         pre = jnp.sum(
             flat[pl.ds(span + s, group, stride=tall), :]
@@ -400,44 +398,82 @@
             keepdims=True,
         ) * own_rms[s]
         live = jnp.where(s < own_len, 1.0, 0.0).astype(f32)
-        betas.append(live * jax.nn.sigmoid(pre[:, :HEADS]))
         arg = pre[:, HEADS : 2 * HEADS] + bias[...]
         soft = jnp.maximum(arg, 0.0) + jnp.log1p(jnp.exp(-jnp.abs(arg)))
-        decays.append(jnp.exp(-live * rate[...] * soft))
+        at = 2 * SLOTS * HEADS + s
+        qk[at : at + 1, 0:HEADS] = live * jax.nn.sigmoid(pre[:, :HEADS])
+        qk[at + SLOTS : at + SLOTS + 1, 0:HEADS] = jnp.exp(-live * rate[...] * soft)
+    qkt[...] = qk[...].T
     inv = HEAD**-0.5
-    state_copies = []
+    many = SLOTS * HEADS
+
+    def start(s, h):
+        return (s * hh + h) * group
+
     for src in range(group):
         for h in range(hh):
-            n = src * hh + h
-            S = st[n]
-            for s in range(SLOTS):
-                col = (s * hh + h) * group + src
-                kc = qkt[:, col + SLOTS * HEADS : col + SLOTS * HEADS + 1]
-                qc = qkt[:, col : col + 1]
-                v = flat[src * tall + s * per + 2 * hh + h : src * tall + s * per + 2 * hh + h + 1, :]
-                S = S * decays[s][:, n : n + 1]
-                recalled = jnp.sum(S * kc, axis=0, keepdims=True)
-                change = betas[s][:, n : n + 1] * (v - recalled)
-                S = S + kc * change
-                outs[col : col + 1, :] = jnp.sum(S * qc, axis=0, keepdims=True) * inv
-            state_out[n] = S
-    for s in range(SLOTS):
-        for h in range(hh):
-            at = (s * hh + h) * group
-            o = outs[at : at + group, :]
+            every = pl.ds(start(0, h) + src, 8, stride=HEADS)
+            flat2[every, :] = jnp.dot(
+                qk[every, :],
+                st[src * hh + h],
+                precision=lax.Precision.HIGHEST,
+                preferred_element_type=f32,
+            )
+
+    def dots(x, y):
+        return jnp.sum(x * y, axis=1, keepdims=True)
+
+    for h in range(hh):
+        per_head = qkt[pl.ds(h, group, stride=hh), :]
+        q, k, seen_q, seen_k, w = [], [], [], [], []
+        beta = [per_head[:, 2 * many + s : 2 * many + s + 1] for s in range(SLOTS)]
+        keep = [
+            per_head[:, 2 * many + SLOTS + s : 2 * many + SLOTS + s + 1] for s in range(SLOTS)
+        ]
+        for s in range(SLOTS):
+            at = start(s, h)
+            q.append(qk[at : at + group, :])
+            k.append(qk[at + many : at + many + group, :])
+            seen_q.append(flat2[at : at + group, :])
+            seen_k.append(flat2[at + many : at + many + group, :])
+        total = jnp.ones((group, 1), f32)
+        for s in range(SLOTS):
+            total = total * keep[s]
+            recalled = total * seen_k[s]
+            w = [keep[s] * x for x in w]
+            for n in range(s):
+                recalled = recalled + dots(k[n], k[s]) * w[n]
+            w.append(beta[s] * (tile(s, 2, h) - recalled))
+            o = total * seen_q[s]
+            for n in range(s + 1):
+                o = o + dots(k[n], q[s]) * w[n]
+            o = o * inv
             z = tile(s, 3, h)
-            gated = (
+            at = start(s, h)
+            outs[at : at + group, :] = (
                 o
                 * lax.rsqrt(jnp.mean(o * o, axis=1, keepdims=True) + EPS)
                 * head_gain[...]
                 * (z * jax.nn.sigmoid(z))
             )
-            outs[at : at + group, :] = gated
+        for s in range(SLOTS):
+            at = 2 * many + start(s, h)
+            flat2[at : at + group, :] = w[s]
+        at = 2 * many + start(SLOTS, h)
+        flat2[at : at + group, :] = jnp.broadcast_to(total, (group, HEAD))
     gx[...] = outs[...].astype(bf16)
     for i, j in others:
         kv, tp = near(i), lax.rem(t + j, 2)
         sends.append(send(gx, rg.at[me], g_send.at[i * 2 + j], g_recv.at[me], kv, tp))
     rg[me] = gx[...]
+    for src in range(group):
+        for h in range(hh):
+            at = 2 * many + start(SLOTS, h) + src
+            S = st[src * hh + h] * flat2[at : at + 1, :]
+            for s in range(SLOTS):
+                col = start(s, h) + src + many
+                S = S + qkt[:, col : col + 1] * flat2[col + many : col + many + 1, :]
+            state_out[src * hh + h] = S
     load_p.wait()
     for i, j in others:
         src = near(i) * 2 + lax.rem(t + j, 2)

time: 35.4 us -> 34.2 us (0.966)
  Pallas kernels: 34.5 us -> 33.3 us
    pallas_call x1, Pallas kernels: 33.5 us -> 32.3 us  [fused(): pl.pallas_call(functools.partial(layer_kernel, nk), out_shape=(pltpu.VMEM...]
where the time goes in v3:
time: 34.2 us; the launch traced here: 33.9 us
  Pallas kernels  33.3 us (97%)
  between operations  0.65 us (2%)
    pallas_call x1, Pallas kernels, fused(): pl.pallas_call(functools.partial(layer_kernel, nk), out_shape=(pltpu.VMEM...  32.3 us
    pallas_call x1, Pallas kernels, fused(): pl.pallas_call(write_kernel, out_shape=(jax.ShapeDtypeStruct((rows, piece...  0.99 us

profile of v3, /device:TPU:0, one launch (start us, length us, event | category | flops | bytes accessed | tf_op | source)
XLA Modules:
  0.0 33.9 jit_solution(797740322519937922)
XLA Ops:
  0.6 32.3 %layer.1 = (bf16[24,512]{1,0:T(8,128)(2,1)S(1)}, f32[16,128,128]{2,1,0:T(8,128)S(1)}) custom-call(bf16[24,512]{1,0:T(8,128)(2,1)} %bitcast.16, s32[8]{0:T(128)} %lengths_hbm.1, f32[16,128,128]{2,1,0:T(8,128)} %bitcast.13, f32[1,4096]{1,0:T(1,128)} %bitcast.17, bf16[4096,256]{1,0:T(8,128)(2,1)} %wq_hbm.1, bf16[4096,256]{1,0:T(8,128)(2,1)} %wk_hbm.1, ...), custom_call_target="tpu_custom_call" | custom-call | tf_op jit(solution)/shard_map/layer/pallas_call | solution.py:597
  32.9 1.0 %write.1 = (bf16[24,512]{1,0:T(8,128)(2,1)}, f32[16,128,128]{2,1,0:T(8,128)}) custom-call(bf16[24,512]{1,0:T(8,128)(2,1)S(1)} %get-tuple-element.6.a, f32[16,128,128]{2,1,0:T(8,128)S(1)} %get-tuple-element.7.b), custom_call_target="tpu_custom_call" | custom-call | tf_op jit(solution)/shard_map/write/pallas_call | solution.py:679
